TPU v7x, 32 devices: a whole 2x2x4 slice. The times are simulated.
32 devices in a mesh: ep: 8 (over z, x), tp: 4 (over y, core).
Axes of the slice: x: 2, y: 2, z: 4, core: 2. Of those that a mesh axis runs over, the one named last changes fastest.
Arguments:
- tokens: bfloat16 [192, 2048], P('ep'), may hold values from -12 to 12
- state: float32 [192, 16, 128, 256], P('ep', 'tp'), may hold values from -6 to 6
- w_query: bfloat16 [2048, 2048], P(None, 'tp'), may hold values from -0.125 to 0.125
- w_key: bfloat16 [2048, 2048], P(None, 'tp'), may hold values from -0.125 to 0.125
- w_value: bfloat16 [2048, 4096], P(None, 'tp'), may hold values from -0.125 to 0.125
- w_outgate: bfloat16 [2048, 4096], P(None, 'tp'), may hold values from -0.125 to 0.125
- decay_down: bfloat16 [2048, 16], replicated, may hold values from -0.125 to 0.125
- decay_up: bfloat16 [16, 2048], P(None, 'tp'), may hold values from -9 to 9
- decay_bias: float32 [2048], P('tp'), may hold values from -6 to 4
- head_gain: float32 [256], replicated, may hold values from 0.1 to 1.9
- w_output: bfloat16 [4096, 2048], P('tp'), may hold values from -0.09375 to 0.09375
- norm1_gain: float32 [2048], P('tp'), may hold values from 0.1 to 1.9
- route_ids: int32 [192, 6], P('ep'), may hold values from 0 to 31, all different within a row; in each aligned block of 24 rows (0 to 23, 24 to 47, ...) at most 5 rows name the same one
- route_weight: float32 [192, 6], P('ep'), may hold values from 0.1 to 1
- exp_gate: bfloat16 [32, 2048, 512], P('ep', 'tp'), may hold values from -0.125 to 0.125
- exp_up: bfloat16 [32, 2048, 512], P('ep', 'tp'), may hold values from -0.125 to 0.125
- exp_down: bfloat16 [32, 512, 2048], P('ep', None, 'tp'), may hold values from -0.25 to 0.25
- sh_gate: bfloat16 [2048, 512], P('tp'), may hold values from -0.125 to 0.125
- sh_up: bfloat16 [2048, 512], P('tp'), may hold values from -0.125 to 0.125
- sh_down: bfloat16 [512, 2048], P(None, 'tp'), may hold values from -0.25 to 0.25
- norm2_gain: float32 [2048], P('tp'), may hold values from 0.1 to 1.9
Outputs:
- layer_out: bfloat16 [192, 2048], P('ep', 'tp')
Inputs may be any that keep to these rules, and one draw needn't show every extreme that they name: `route_ids`: each row names 6 different experts. Among the rows of one index of ep (aligned blocks of 24 rows) no expert is named by more than 5 rows, and in some blocks one expert is named by exactly 5.
All inputs are finite; a program needn't handle non-finite values.
Results may differ from a plain program's by a relative error of at most 0.02.
Values may be sent and summed in bfloat16 or wider, within the bound.
A program may use at most 64 MiB of HBM per device.

v0:
```python
import functools

import jax
import jax.numpy as jnp
from jax import lax
from jax.experimental import pallas as pl
from jax.experimental.pallas import tpu as pltpu
from jax.sharding import PartitionSpec as P

res_scale = 2.0**0.5
decay_tau = 16.0
norm_eps = 1e-05
AHEAD = 10
F32 = jnp.float32
BF16 = jnp.bfloat16


def dot(left, right):
    return jnp.dot(left, right, preferred_element_type=F32)


def dot_nt(left, right):
    return lax.dot_general(left, right, (((1,), (1,)), ((), ())), preferred_element_type=F32)


def iota_f(shape, dim):
    return lax.broadcasted_iota(jnp.int32, shape, dim).astype(F32)


def quotient(values, divisor):
    return jnp.floor((values + 0.5) * (1.0 / divisor))


def silu(x):
    return x * (1.0 / (1.0 + jnp.exp(-x)))


def kernel(
    dims,
    tokens,
    decay_down,
    decay_up,
    decay_bias,
    head_gain,
    norm1_gain,
    route_ids,
    route_weight,
    norm2_gain,
    state_h,
    wq_h,
    wk_h,
    wv_h,
    wg_h,
    wo_h,
    eg_h,
    eu_h,
    ed_h,
    sg_h,
    su_h,
    sd_h,
    out,
    state,
    wq,
    wk,
    wv,
    wg,
    wo,
    eg,
    eu,
    ed,
    sg,
    su,
    sd,
    dq_ref,
    att_ref,
    head_out,
    p1s,
    p1r,
    p2s,
    p2r,
    p3s,
    p3r,
    p4s,
    p4r,
    p4hs,
    p4hr,
    p5,
    p5h,
    p6s,
    p6r,
    p7s,
    p7r,
    load_sem,
    tp_send,
    tp_recv,
    ep_send,
    ep_recv,
):
    (rows, heads, kdim, vdim, cols, tp, ep, local, cap, rd, groups, fc, fsc, top, chunks) = dims
    experts = local * ep
    slots = ep * rd
    me_t = lax.axis_index("tp")
    me_e = lax.axis_index("ep")

    def tp_peer(offset):
        return lax.rem(me_t + offset, tp)

    def ep_peer(offset):
        return lax.rem(me_e + offset, ep)

    barrier = pltpu.get_barrier_semaphore()
    for offset in range(1, tp):
        pl.semaphore_signal(
            barrier, inc=1, device_id=(me_e, tp_peer(offset)), device_id_type=pl.DeviceIdType.MESH
        )
    for offset in range(1, ep):
        pl.semaphore_signal(
            barrier, inc=1, device_id=(ep_peer(offset), me_t), device_id_type=pl.DeviceIdType.MESH
        )

    loads = []

    def add_load(src, dst):
        loads.append(pltpu.make_async_copy(src, dst, load_sem.at[len(loads)]))
        return len(loads) - 1

    step = rows // chunks
    i_wq = add_load(wq_h, wq)
    i_wk = add_load(wk_h, wk)
    i_state = [
        add_load(state_h.at[pl.ds(c * step, step)], state.at[pl.ds(c * step, step)])
        for c in range(chunks)
    ]
    half = wv_h.shape[0] // 2
    i_wv = [add_load(wv_h.at[pl.ds(c * half, half)], wv.at[pl.ds(c * half, half)]) for c in range(2)]
    i_wg = [add_load(wg_h.at[pl.ds(c * half, half)], wg.at[pl.ds(c * half, half)]) for c in range(2)]
    i_wo = []
    for offset in range(tp):
        start = pl.multiple_of(tp_peer(offset + 1) * cols, 128)
        i_wo.append(add_load(wo_h.at[:, pl.ds(start, cols)], wo.at[offset]))
    i_sg = add_load(sg_h, sg)
    i_su = add_load(su_h, su)
    i_eg = add_load(eg_h, eg)
    i_eu = add_load(eu_h, eu)
    i_sd = add_load(sd_h, sd)
    i_ed = add_load(ed_h, ed)
    for copy in loads[:AHEAD]:
        copy.start()

    def ready(index):
        loads[index].wait()
        if index + AHEAD < len(loads):
            loads[index + AHEAD].start()

    def tp_copy(src, dst, kind, slot, target):
        return pltpu.make_async_remote_copy(
            src_ref=src,
            dst_ref=dst,
            send_sem=tp_send.at[kind, slot],
            recv_sem=tp_recv.at[kind, slot],
            device_id=(me_e, target),
            device_id_type=pl.DeviceIdType.MESH,
        )

    def ep_copy(src, dst, kind, slot, target):
        return pltpu.make_async_remote_copy(
            src_ref=src,
            dst_ref=dst,
            send_sem=ep_send.at[kind, slot],
            recv_sem=ep_recv.at[kind, slot],
            device_id=(target, me_t),
            device_id_type=pl.DeviceIdType.MESH,
        )

    tok = tokens[...]
    decay_low = dot_nt(tok, decay_down[...]).astype(BF16)
    pre = dot(decay_low, decay_up[...]) + decay_bias[...]
    log_decay = (jnp.minimum(pre, 0.0) - jnp.log(1.0 + jnp.exp(-jnp.abs(pre)))) * (1.0 / decay_tau)
    ids = route_ids[...]
    weights = route_weight[...]
    expert_iota = lax.broadcasted_iota(jnp.int32, (experts, rows), 0)
    member = jnp.zeros((experts, rows), F32)
    weight_of = jnp.zeros((experts, rows), F32)
    for k in range(top):
        hit = ids[k : k + 1, :] == expert_iota
        member = jnp.where(hit, 1.0, member)
        weight_of = jnp.where(hit, weights[k : k + 1, :], weight_of)
    member_b = member.astype(BF16)
    earlier = (iota_f((rows, rows), 0) < iota_f((rows, rows), 1)).astype(F32).astype(BF16)
    identity = (iota_f((rows, rows), 0) == iota_f((rows, rows), 1)).astype(F32).astype(BF16)
    rank_b = dot(member_b, earlier).astype(BF16)

    def slot_parts(number):
        dest = quotient(number, rd)
        inner = number - dest * rd
        which = quotient(inner, cap)
        return dest * local + which, inner - which * cap, which, inner < local * cap

    e_col, c_col, _, ok_col = slot_parts(iota_f((slots, 1), 0))
    expand = ((iota_f((slots, experts), 1) == e_col) & ok_col).astype(F32).astype(BF16)
    placed = (dot(expand, member_b) > 0.5) & (dot(expand, rank_b) == c_col)
    place = jnp.where(placed, 1.0, 0.0).astype(BF16)
    weight_hi = weight_of.astype(BF16)
    weight_lo = (weight_of - weight_hi.astype(F32)).astype(BF16)
    spread_hi = jnp.where(placed, dot(expand, weight_hi), 0.0).astype(BF16)
    spread_lo = jnp.where(placed, dot(expand, weight_lo), 0.0).astype(BF16)
    per = ep * cap
    packed = local * per

    def packed_slot(number):
        which = quotient(number, per)
        inner = number - which * per
        source = quotient(inner, cap)
        return source * rd + which * cap + inner - source * cap

    squeeze = packed_slot(iota_f((packed, slots), 0)) == iota_f((packed, slots), 1)
    squeeze = jnp.where(squeeze, 1.0, 0.0).astype(BF16)
    widen = packed_slot(iota_f((slots, packed), 1)) == iota_f((slots, packed), 0)
    widen = jnp.where(widen, 1.0, 0.0).astype(BF16)
    gather_hi = dot_nt(identity, spread_hi).astype(BF16)
    gather_lo = dot_nt(identity, spread_lo).astype(BF16)

    ready(i_wq)
    queries = dot(tok, wq[...]).astype(BF16).astype(F32) * kdim ** (-0.5)
    dq_ref[...] = queries * jnp.exp(log_decay)
    ready(i_wk)
    key_rows = dot(tok, wk[...]).astype(BF16).astype(F32)
    pairs = queries * key_rows
    width = heads * kdim
    hr = att_ref.shape[1]
    head_mask = quotient(iota_f((hr, width), 1), kdim) == iota_f((hr, width), 0)
    for c in range(chunks):
        ready(i_state[c])

        def one_row(b, carry):
            left = jnp.where(head_mask, dq_ref[pl.ds(b, 1), :], 0.0).astype(BF16)
            right = state[b].reshape(width, vdim).astype(BF16)
            att_ref[b] = dot(left, right)
            return carry

        lax.fori_loop(c * step, (c + 1) * step, one_row, 0, unroll=min(step, 3))
    for i in i_wv:
        ready(i)
    values = dot(tok, wv[...]).astype(BF16).astype(F32)
    for i in i_wg:
        ready(i)
    gate_pre = dot(tok, wg[...]).astype(BF16).astype(F32)
    for h in range(heads):
        part = slice(h * vdim, (h + 1) * vdim)
        score = jnp.sum(pairs[:, h * kdim : (h + 1) * kdim], -1, keepdims=True)
        attended = att_ref[:, h, :] + score * values[:, part]
        inv = lax.rsqrt(jnp.mean(attended * attended, -1, keepdims=True) + norm_eps)
        head_out[:, part] = (attended * inv * head_gain[...] * silu(gate_pre[:, part])).astype(BF16)
    pl.semaphore_wait(barrier, tp - 1 + ep - 1)

    sent = []
    heads_side = head_out[...]
    own = None
    for offset in range(1, tp + 1):
        ready(i_wo[offset - 1])
        product = dot(heads_side, wo[offset - 1])
        if offset < tp:
            p1s[offset] = product.astype(BF16)
            copy = tp_copy(p1s.at[offset], p1r.at[offset], 0, offset, tp_peer(offset))
            copy.start()
            sent.append(copy)
        else:
            own = product
    start = pl.multiple_of(me_t * cols, 128)
    resid = own + res_scale * tokens[:, pl.ds(start, cols)].astype(F32)
    for offset in range(1, tp):
        sent[offset - 1].wait_recv()
        resid = resid + p1r[offset].astype(F32)

    def layer_norm(values, send_ref, recv_ref, kind, gain):
        mean = jnp.mean(values, -1, keepdims=True)
        center = values - mean
        moment = jnp.sum(center * center, -1, keepdims=True)
        lane = lax.broadcasted_iota(jnp.int32, (rows, 128), 1)
        send_ref[...] = jnp.where(lane == 0, mean, moment)
        copies = []
        for offset in range(1, tp):
            copy = tp_copy(send_ref, recv_ref.at[offset], kind, offset, tp_peer(offset))
            copy.start()
            copies.append(copy)
        sent.extend(copies)
        means, moments = [mean], moment
        for offset in range(1, tp):
            copies[offset - 1].wait_recv()
            tile = recv_ref[offset]
            means.append(tile[:, 0:1])
            moments = moments + tile[:, 1:2]
        total = sum(means) * (1.0 / tp)
        for m in means:
            moments = moments + cols * (m - total) * (m - total)
        return (values - total) * lax.rsqrt(moments * (1.0 / (cols * tp)) + norm_eps) * gain[...]

    normed = layer_norm(resid, p2s, p2r, 1, norm1_gain).astype(BF16)

    p3s[...] = dot(place, normed).astype(BF16).reshape(ep, rd, cols)
    routed_copies = []
    for offset in sorted(range(1, ep), key=lambda o: -min(o, ep - o)):
        target = ep_peer(offset)
        copy = ep_copy(p3s.at[target], p3r.at[offset], 0, offset, target)
        copy.start()
        routed_copies.append(copy)
    sent.extend(routed_copies)
    p3r[0] = p3s[me_e]

    def send_rows(send_ref, recv_ref, kind, group):
        @pl.when(me_t != group)
        def _():
            pltpu.make_async_remote_copy(
                src_ref=send_ref.at[group],
                dst_ref=recv_ref.at[me_t],
                send_sem=tp_send.at[kind, group],
                recv_sem=tp_recv.at[kind, me_t],
                device_id=(me_e, group),
                device_id_type=pl.DeviceIdType.MESH,
            ).start()

    def settle_sends(send_ref, recv_ref, kind):
        for group in range(groups):

            @pl.when(me_t != group)
            def _():
                tp_copy(send_ref.at[group], recv_ref.at[me_t], kind, group, group).wait_send()

    ready(i_sg)
    ready(i_su)
    shared_gate, shared_up = dot(normed, sg[...]), dot(normed, su[...])
    for group in range(groups):
        part = slice(group * fsc, (group + 1) * fsc)
        p4hs[group, :, 0:fsc] = shared_gate[:, part].astype(BF16)
        p4hs[group, :, fsc : 2 * fsc] = shared_up[:, part].astype(BF16)
        send_rows(p4hs, p4hr, 3, group)

    ready(i_eg)
    ready(i_eu)
    for copy in routed_copies:
        copy.wait_recv()
    incoming = dot(squeeze, p3r[...].reshape(slots, cols))
    chosen = [incoming[e * per : (e + 1) * per].astype(BF16) for e in range(local)]
    slab = 2 if groups % 2 == 0 else 1
    for first in range(0, groups, slab):
        part = slice(first * fc, (first + slab) * fc)
        for e in range(local):
            at = slice(e * per, (e + 1) * per)
            gate_sum = dot(chosen[e], eg[e, :, part])
            up_sum = dot(chosen[e], eu[e, :, part])
            for i in range(slab):
                cut = slice(i * fc, (i + 1) * fc)
                p4s[first + i, at, 0:fc] = gate_sum[:, cut].astype(BF16)
                p4s[first + i, at, fc : 2 * fc] = up_sum[:, cut].astype(BF16)
        for i in range(slab):
            send_rows(p4s, p4r, 2, first + i)

    def reduce(send_ref, recv_ref, kind, dest, kind_out, chunk):
        total = send_ref[me_t].astype(F32)
        for offset in range(1, tp):
            source = tp_peer(offset)
            tp_copy(send_ref.at[0], recv_ref.at[source], kind, source, source).wait_recv()
            total = total + recv_ref[source].astype(F32)
        dest[me_t] = (silu(total[:, 0:chunk]) * total[:, chunk : 2 * chunk]).astype(BF16)
        for offset in range(1, tp):
            pltpu.make_async_remote_copy(
                src_ref=dest.at[me_t],
                dst_ref=dest.at[me_t],
                send_sem=tp_send.at[kind_out, offset],
                recv_sem=tp_recv.at[kind_out, me_t],
                device_id=(me_e, tp_peer(offset)),
                device_id_type=pl.DeviceIdType.MESH,
            ).start()

    def all_reduce():
        reduce(p4hs, p4hr, 3, p5h, 5, fsc)
        reduce(p4s, p4r, 2, p5, 4, fc)

    def gathered(dest, kind):
        for group in range(groups):

            @pl.when(me_t != group)
            def _():
                tp_copy(dest.at[group], dest.at[group], kind, group, group).wait_recv()

    if groups == tp:
        all_reduce()
    else:
        pl.when(me_t < groups)(all_reduce)
    settle_sends(p4hs, p4hr, 3)
    settle_sends(p4s, p4r, 2)
    gathered(p5h, 5)
    ready(i_sd)
    mixture = sum(
        dot(p5h[group], sd[group * fsc : (group + 1) * fsc, :]) for group in range(groups)
    )
    ready(i_ed)
    gathered(p5, 4)
    inner = jnp.concatenate([p5[group] for group in range(groups)], 1).astype(F32)
    answer = jnp.concatenate(
        [dot(inner[e * per : (e + 1) * per].astype(BF16), ed[e]) for e in range(local)], 0
    ).astype(BF16)
    p6s[...] = dot(widen, answer).astype(BF16).reshape(ep, rd, cols)
    back_copies = []
    for offset in sorted(range(1, ep), key=lambda o: -min(o, ep - o)):
        source = ep_peer(ep - offset)
        copy = ep_copy(p6s.at[offset], p6r.at[ep_peer(0)], 1, offset, source)
        copy.start()
        back_copies.append(copy)
    sent.extend(back_copies)
    p6r[me_e] = p6s[0]
    for offset in range(1, ep):
        expert_dev = ep_peer(offset)
        ep_copy(p6s.at[offset], p6r.at[expert_dev], 1, offset, expert_dev).wait_recv()
    returned = p6r[...].reshape(slots, cols)
    mixture = mixture + dot(gather_hi, returned) + dot(gather_lo, returned)
    last = res_scale * normed.astype(F32) + mixture
    out[...] = layer_norm(last, p7s, p7r, 6, norm2_gain).astype(BF16)
    for copy in sent:
        copy.wait_send()

    def settle_gather(dest, kind):
        for offset in range(1, tp):
            tp_copy(dest.at[me_t], dest.at[me_t], kind, offset, tp_peer(offset)).wait_send()

    def settle_gathers():
        settle_gather(p5, 4)
        settle_gather(p5h, 5)

    if groups == tp:
        settle_gathers()
    else:
        pl.when(me_t < groups)(settle_gathers)


def per_device(
    tokens,
    state,
    w_query,
    w_key,
    w_value,
    w_outgate,
    decay_down,
    decay_up,
    decay_bias,
    head_gain,
    w_output,
    norm1_gain,
    route_ids,
    route_weight,
    exp_gate,
    exp_up,
    exp_down,
    sh_gate,
    sh_up,
    sh_down,
    norm2_gain,
):
    rows, width = tokens.shape
    heads, kdim, vdim = state.shape[1:]
    tp, ep = lax.axis_size("tp"), lax.axis_size("ep")
    cols = width // tp
    top = route_ids.shape[1]
    local = exp_gate.shape[0]
    cap = max(2, rows * top // (local * ep) + 1)
    rd = -(-local * cap // 8) * 8
    packed = local * cap * ep
    ff, fs = exp_gate.shape[2], sh_gate.shape[1]
    groups = min(tp, ff // 128, fs // 128)
    fc, fsc = ff // groups, fs // groups
    chunks = 4
    dims = (rows, heads, kdim, vdim, cols, tp, ep, local, cap, rd, groups, fc, fsc, top, chunks)
    n_loads = 2 + chunks + 4 + tp + 6
    vm = pltpu.VMEM
    vmem = pl.BlockSpec(memory_space=pltpu.VMEM)
    hbm = pl.BlockSpec(memory_space=pl.ANY)
    return pl.pallas_call(
        functools.partial(kernel, dims),
        out_shape=jax.ShapeDtypeStruct((rows, cols), BF16),
        in_specs=[vmem] * 9 + [hbm] * 12,
        out_specs=vmem,
        scratch_shapes=[
            vm(state.shape, F32),
            vm(w_query.shape, BF16),
            vm(w_key.shape, BF16),
            vm(w_value.shape, BF16),
            vm(w_outgate.shape, BF16),
            vm((tp, w_output.shape[0], cols), BF16),
            vm(exp_gate.shape, BF16),
            vm(exp_up.shape, BF16),
            vm(exp_down.shape, BF16),
            vm(sh_gate.shape, BF16),
            vm(sh_up.shape, BF16),
            vm(sh_down.shape, BF16),
            vm((rows, heads * kdim), F32),
            vm((rows, -(-heads // 8) * 8, vdim), F32),
            vm((rows, heads * vdim), BF16),
            vm((tp, rows, cols), BF16),
            vm((tp, rows, cols), BF16),
            vm((rows, 128), F32),
            vm((tp, rows, 128), F32),
            vm((ep, rd, cols), BF16),
            vm((ep, rd, cols), BF16),
            vm((groups, packed, 2 * fc), BF16),
            vm((tp, packed, 2 * fc), BF16),
            vm((groups, rows, 2 * fsc), BF16),
            vm((tp, rows, 2 * fsc), BF16),
            vm((groups, packed, fc), BF16),
            vm((groups, rows, fsc), BF16),
            vm((ep, rd, cols), BF16),
            vm((ep, rd, cols), BF16),
            vm((rows, 128), F32),
            vm((tp, rows, 128), F32),
            pltpu.SemaphoreType.DMA((n_loads,)),
            pltpu.SemaphoreType.DMA((7, tp)),
            pltpu.SemaphoreType.DMA((7, tp)),
            pltpu.SemaphoreType.DMA((2, ep)),
            pltpu.SemaphoreType.DMA((2, ep)),
        ],
        compiler_params=pltpu.CompilerParams(
            collective_id=0, has_side_effects=True, vmem_limit_bytes=60 * 1024 * 1024
        ),
        name="layer",
    )(
        tokens,
        decay_down.T,
        decay_up,
        decay_bias[None, :],
        head_gain[None, :],
        norm1_gain[None, :],
        route_ids.T,
        route_weight.T,
        norm2_gain[None, :],
        state,
        w_query,
        w_key,
        w_value,
        w_outgate,
        w_output,
        exp_gate,
        exp_up,
        exp_down,
        sh_gate,
        sh_up,
        sh_down,
    )


def solution(mesh):
    in_specs = (
        P("ep", None),
        P("ep", "tp", None, None),
        P(None, "tp"),
        P(None, "tp"),
        P(None, "tp"),
        P(None, "tp"),
        P(),
        P(None, "tp"),
        P("tp"),
        P(),
        P("tp", None),
        P("tp"),
        P("ep", None),
        P("ep", None),
        P("ep", "tp", None),
        P("ep", "tp", None),
        P("ep", None, "tp"),
        P("tp", None),
        P("tp", None),
        P(None, "tp"),
        P("tp"),
    )
    out_specs = P("ep", "tp")
    return jax.shard_map(
        per_device, mesh=mesh, in_specs=in_specs, out_specs=out_specs, check_vma=False
    )
```

profile of v0, /device:TPU:0, one launch (start us, length us, event | category | flops | bytes accessed | tf_op | source)
XLA Modules:
  0.0 48.0 jit_solution(9104490072037220510)
XLA Ops:
  0.0 46.6 %layer.1 = bf16[24,512]{1,0:T(8,128)(2,1)} custom-call(bf16[24,2048]{1,0:T(8,128)(2,1)} %tokens.1, bf16[16,2048]{1,0:T(8,128)(2,1)} %bitcast.7, bf16[16,512]{1,0:T(8,128)(2,1)} %decay_up.1, f32[1,512]{1,0:T(1,128)} %bitcast.10, f32[1,256]{1,0:T(1,128)} %bitcast.13, f32[1,512]{1,0:T(1,128)} %bitcast.11, s32[6,24]{1,0:T(8,128)} %bitcast.8, f32[6,24]{1,0:T(8,128)} %bitcast.9, ...), custom_call_target="tpu_custom_call" | custom-call | tf_op jit(solution)/shard_map/layer/pallas_call | solution.py:477
  46.6 1.3 %copy.23 = bf16[24,512]{1,0:T(8,128)(2,1)} copy(bf16[24,512]{1,0:T(8,128)(2,1)} %layer.1) | data formatting | bytes 49152
where the time goes:
time: 48.2 us; the launch traced here: 48 us
  Pallas kernels  46.6 us (97%)
  local copies, waits for them, and re-layouts  1.35 us (3%)
    pallas_call x1, Pallas kernels, per_device(): pl.pallas_call(functools.partial(kernel, dims), out_shape=jax.ShapeDtypeS...  46.6 us
    unnamed x1, local copies, waits for them, and re-layouts  1.35 us

commit v1 on v0

v1 whole, which is shorter than its diff:
```python
import functools

import jax
import jax.numpy as jnp
from jax import lax
from jax.experimental import pallas as pl
from jax.experimental.pallas import tpu as pltpu
from jax.sharding import PartitionSpec as P

res_scale = 2.0**0.5
decay_tau = 16.0
norm_eps = 1e-05
AHEAD = 10
F32 = jnp.float32
BF16 = jnp.bfloat16


def dot(left, right):
    return jnp.dot(left, right, preferred_element_type=F32)


def dot_nt(left, right):
    return lax.dot_general(left, right, (((1,), (1,)), ((), ())), preferred_element_type=F32)


def iota(shape, dim):
    return lax.broadcasted_iota(jnp.int32, shape, dim)


def iota_f(shape, dim):
    return iota(shape, dim).astype(F32)


def quotient(values, divisor):
    return jnp.floor((values + 0.5) * (1.0 / divisor))


def ones_where(mask):
    return jnp.where(mask, 1.0, 0.0)


def silu(x):
    return x * (1.0 / (1.0 + jnp.exp(-x)))


def pad_to(n, multiple):
    return -(-n // multiple) * multiple


def bands(count, per):
    return [(e * per // 8 * 8, pad_to((e + 1) * per, 8)) for e in range(count)]


def join_bands(pieces, per):
    spans = bands(len(pieces), per)
    tiles = []
    for row in range(0, spans[-1][1], 8):
        tile = None
        for e, (first, last) in enumerate(spans):
            if first <= row < last:
                part = pieces[e][row - first : row - first + 8]
                if tile is None:
                    tile = part
                else:
                    tile = jnp.where(iota((8, 1), 0) + row < e * per, tile, part)
        tiles.append(tile)
    return jnp.concatenate(tiles, 0)


def kernel(dims, *refs):
    (rows, heads, kdim, vdim, width, cols, tp, ep, local, cap, top, ff, fs, chunks, nch, r16) = dims
    (tok_h, dd_h, du_h, db_h, hg_h, g1_h, ids_h, rw_h, g2_h) = refs[0:9]
    (state_h, wq_h, wk_h, wv_h, wg_h, wo_h, eg_h, eu_h, ed_h, sg_h, su_h, sd_h) = refs[9:21]
    out = refs[21]
    (tok_v, dd_v, du_v, db_v, hg_v, g1_v, ids_v, rw_v, g2_v) = refs[22:31]
    (state, wq, wk, wv, wg, wo, eg, eu, ed, sg, su, sd) = refs[31:43]
    (dq_ref, att_ref, head_out, val_s, route_s, route_r, pick, give_hi, give_lo) = refs[43:52]
    (p1s, p1r, sum_s, sum_r, sq_s, sq_r, ln_s, ln_r, inv_s, inv_r, xs, xr) = refs[52:64]
    (es, er, eo, ys, yr, inner) = refs[64:70]
    (hs, hr, ho, hys, hyr, hinner) = refs[70:76]
    (bs, br) = refs[76:78]
    (load_sem, tp_send, tp_recv, ep_send, ep_recv) = refs[78:83]

    experts = local * ep
    ny = tp // 2
    ns = ep // nch
    per = ns * cap
    slots = local * per
    lanes = ns * rows
    hf, hfs = ff // 2, fs // 2
    me_t = lax.axis_index("tp")
    me_e = lax.axis_index("ep")
    me_c = lax.rem(me_t, 2)

    def tp_peer(i, f):
        return lax.rem(me_t - me_c + 2 * i, tp) + me_c + f * (1 - 2 * me_c)

    def ep_peer(offset):
        return lax.rem(me_e + offset, ep)

    barrier = pltpu.get_barrier_semaphore()
    loads = []

    def add_load(src, dst):
        loads.append(pltpu.make_async_copy(src, dst, load_sem.at[len(loads)]))
        return len(loads) - 1

    i_tok = add_load(tok_h, tok_v)
    i_dd = add_load(dd_h, dd_v)
    i_wq = add_load(wq_h, wq)
    i_small = [
        add_load(src, dst)
        for src, dst in zip(
            (du_h, db_h, ids_h, rw_h, hg_h, g1_h, g2_h),
            (du_v, db_v, ids_v, rw_v, hg_v, g1_v, g2_v),
        )
    ]
    i_wk = add_load(wk_h, wk)
    step = rows // chunks
    i_state = [
        add_load(state_h.at[pl.ds(c * step, step)], state.at[pl.ds(c * step, step)])
        for c in range(chunks)
    ]
    half = wv_h.shape[0] // 2
    i_wv = [add_load(wv_h.at[pl.ds(c * half, half)], wv.at[pl.ds(c * half, half)]) for c in range(2)]
    i_wg = [add_load(wg_h.at[pl.ds(c * half, half)], wg.at[pl.ds(c * half, half)]) for c in range(2)]
    tp_order = [(i, f) for i in range(1, ny) for f in range(2)] + [(0, 1), (0, 0)]
    i_wo = []
    for n, (i, f) in enumerate(tp_order):
        start = pl.multiple_of(tp_peer(i, f) * cols, 128)
        i_wo.append(add_load(wo_h.at[:, pl.ds(start, cols)], wo.at[n]))
    i_sg = add_load(sg_h, sg)
    i_su = add_load(su_h, su)
    i_eg = add_load(eg_h, eg)
    i_eu = add_load(eu_h, eu)
    i_sd = add_load(sd_h, sd)
    i_ed = add_load(ed_h, ed)
    ahead = AHEAD + 10
    for copy in loads[:ahead]:
        copy.start()

    def ready(index):
        loads[index].wait()
        if index + ahead < len(loads):
            loads[index + ahead].start()

    for i, f in tp_order[:-1]:
        pl.semaphore_signal(
            barrier, inc=1, device_id=(me_e, tp_peer(i, f)), device_id_type=pl.DeviceIdType.MESH
        )
    for offset in range(1, ep):
        pl.semaphore_signal(
            barrier, inc=1, device_id=(ep_peer(offset), me_t), device_id_type=pl.DeviceIdType.MESH
        )

    sent = []

    def tp_copy(src, dst, kind, i, f):
        return pltpu.make_async_remote_copy(
            src_ref=src,
            dst_ref=dst,
            send_sem=tp_send.at[kind, 2 * i + f],
            recv_sem=tp_recv.at[kind, 2 * i + f],
            device_id=(me_e, tp_peer(i, f)),
            device_id_type=pl.DeviceIdType.MESH,
        )

    def tp_start(src, dst, kind, i, f):
        copy = tp_copy(src, dst, kind, i, f)
        copy.start()
        sent.append(copy)
        return copy

    def ep_start(src, dst, kind, slot, offset):
        copy = pltpu.make_async_remote_copy(
            src_ref=src,
            dst_ref=dst,
            send_sem=ep_send.at[kind, slot],
            recv_sem=ep_recv.at[kind, slot],
            device_id=(ep_peer(offset), me_t),
            device_id_type=pl.DeviceIdType.MESH,
        )
        copy.start()
        sent.append(copy)
        return copy

    def to_row(col, spread, shift):
        mask = iota((rows, spread), 1) == iota((rows, spread), 0) + shift
        return jnp.sum(jnp.where(mask, col, 0.0), 0, keepdims=True)

    def to_col(row):
        mask = iota((rows, row.shape[1]), 1) == iota((rows, row.shape[1]), 0)
        return jnp.sum(jnp.where(mask, row, 0.0), 1, keepdims=True)

    ready(i_tok)
    ready(i_dd)
    tok = tok_v[...]
    decay_low = dot_nt(tok, dd_v[...]).astype(BF16)
    ready(i_wq)
    queries = dot(tok, wq[...]).astype(BF16).astype(F32) * kdim ** (-0.5)
    for i in i_small:
        ready(i)
    pre = dot(decay_low, du_v[...]) + db_v[...]
    log_decay = (jnp.minimum(pre, 0.0) - jnp.log(1.0 + jnp.exp(-jnp.abs(pre)))) * (1.0 / decay_tau)
    dq_ref[...] = queries * jnp.exp(log_decay)

    ids = ids_v[...]
    weights = rw_v[...]
    line = iota_f((ep * r16, rows), 0)
    line_dev = quotient(line, r16)
    line_in = line - line_dev * r16
    line_kind = quotient(line_in, local)
    line_expert = (line_dev * local + line_in - line_kind * local).astype(jnp.int32)
    member = jnp.zeros((ep * r16, rows), F32)
    weight_of = jnp.zeros((ep * r16, rows), F32)
    for k in range(top):
        hit = ids[k : k + 1, :] == line_expert
        member = jnp.where(hit, 1.0, member)
        weight_of = jnp.where(hit, weights[k : k + 1, :], weight_of)
    earlier = ones_where(iota((rows, rows), 0) < iota((rows, rows), 1)).astype(BF16)
    rank = dot(member.astype(BF16), earlier)
    weight_hi = weight_of.astype(BF16).astype(F32)
    packed = jnp.where(line_kind == 0.0, member * (rank + 1.0), 0.0)
    packed = jnp.where(line_kind == 1.0, weight_hi, packed)
    packed = jnp.where(line_kind == 2.0, weight_of - weight_hi, packed)
    val_s[...] = packed.reshape(ep, r16, rows)
    spread_w = route_s.shape[2]
    for offset in range(ep):
        shift = offset // nch * rows
        spread = ones_where(iota((rows, spread_w), 1) == iota((rows, spread_w), 0) + shift)
        route_s[offset] = dot(val_s[ep_peer(offset)].astype(BF16), spread.astype(BF16)).astype(BF16)

    ready(i_wk)
    key_rows = dot(tok, wk[...]).astype(BF16).astype(F32)
    pairs = queries * key_rows
    key_width = heads * kdim
    hr_pad = att_ref.shape[1]
    head_mask = quotient(iota_f((hr_pad, key_width), 1), kdim) == iota_f((hr_pad, key_width), 0)
    far_first = sorted(range(1, ep), key=lambda o: (o % nch, -min(o, ep - o)))
    route_copies = []
    for c in range(chunks):
        ready(i_state[c])

        def one_row(b, carry):
            left = jnp.where(head_mask, dq_ref[pl.ds(b, 1), :], 0.0).astype(BF16)
            right = state[b].reshape(key_width, vdim).astype(BF16)
            att_ref[b] = dot(left, right)
            return carry

        lax.fori_loop(c * step, (c + 1) * step, one_row, 0, unroll=min(step, 3))
        if c == 0:
            pl.semaphore_wait(barrier, tp - 1 + ep - 1)
            route_r[0] = route_s[0]
            for offset in far_first:
                route_copies.append(
                    ep_start(route_s.at[offset], route_r.at[offset], 0, offset, offset)
                )
    for i in i_wv:
        ready(i)
    values = dot(tok, wv[...]).astype(BF16).astype(F32)
    for i in i_wg:
        ready(i)
    gate_pre = dot(tok, wg[...]).astype(BF16).astype(F32)
    for h in range(heads):
        part = slice(h * vdim, (h + 1) * vdim)
        score = jnp.sum(pairs[:, h * kdim : (h + 1) * kdim], -1, keepdims=True)
        attended = att_ref[:, h, :] + score * values[:, part]
        inv = lax.rsqrt(jnp.mean(attended * attended, -1, keepdims=True) + norm_eps)
        head_out[:, part] = (attended * inv * hg_v[...] * silu(gate_pre[:, part])).astype(BF16)

    heads_side = head_out[...]
    own, total_cols = None, None
    for n, (i, f) in enumerate(tp_order):
        ready(i_wo[n])
        product = dot(heads_side, wo[n])
        if (i, f) == (0, 0):
            own = product
        else:
            rounded = product.astype(BF16)
            p1s[n] = rounded
            tp_start(p1s.at[n], p1r.at[n], 0, i, f)
            product = rounded.astype(F32)
        total_cols = product if total_cols is None else total_cols + product
    row_sum = to_row(jnp.sum(total_cols, -1, keepdims=True), sum_s.shape[1], 0)
    sum_s[...] = jnp.broadcast_to(row_sum, sum_s.shape)
    for n, (i, f) in enumerate(tp_order[:-1]):
        tp_start(sum_s, sum_r.at[n], 1, i, f)

    for copy in route_copies:
        copy.wait_recv()
    slot_f = iota_f((slots, lanes), 0)
    slot_expert = quotient(slot_f, per)
    slot_in = slot_f - slot_expert * per
    slot_source = quotient(slot_in, cap)
    slot_code = slot_in - slot_source * cap + 1.0
    same_source = quotient(iota_f((slots, lanes), 1), rows) == slot_source
    eye = ones_where(iota((lanes, lanes), 0) == iota((lanes, lanes), 1)).astype(BF16)
    for p in range(nch):
        table = route_r[p].astype(F32)
        for q in range(1, ns):
            table = table + route_r[q * nch + p].astype(F32)
        table = table[:, 0:lanes]

        def rows_of(kind):
            spread = jnp.zeros((slots, lanes), F32)
            for k in range(local):
                line_at = kind * local + k
                spread = jnp.where(slot_expert == k, table[line_at : line_at + 1, :], spread)
            return spread

        placed = (rows_of(0) == slot_code) & same_source
        pick[p] = ones_where(placed).astype(BF16)
        give_hi[p] = dot_nt(eye, jnp.where(placed, rows_of(1), 0.0).astype(BF16)).astype(BF16)
        give_lo[p] = dot_nt(eye, jnp.where(placed, rows_of(2), 0.0).astype(BF16)).astype(BF16)

    start = pl.multiple_of(me_t * cols, 128)
    resid = own + res_scale * tok_v[:, pl.ds(start, cols)].astype(F32)
    token_sum = res_scale * jnp.sum(tok.astype(F32), -1, keepdims=True)
    for n, (i, f) in enumerate(tp_order[:-1]):
        tp_copy(p1s.at[n], p1r.at[n], 0, i, f).wait_recv()
        resid = resid + p1r[n].astype(F32)
    for n, (i, f) in enumerate(tp_order[:-1]):
        tp_copy(sum_s, sum_r.at[n], 1, i, f).wait_recv()
        row_sum = row_sum + sum_r[n][0:1, :]
    mean = (to_col(row_sum) + token_sum) * (1.0 / width)
    center = resid - mean
    gained = center * g1_v[...]
    xs[...] = gained.astype(BF16)
    x_copies = {}
    for offset in far_first:
        x_copies[offset] = ep_start(xs, xr.at[offset % nch, offset // nch], 1, offset, offset)
    xr[0, 0] = xs[...]
    squares = to_row(jnp.sum(center * center, -1, keepdims=True), sq_s.shape[1], 0)
    sq_s[...] = jnp.broadcast_to(squares, sq_s.shape)
    for n, (i, f) in enumerate(tp_order[:-1]):
        tp_start(sq_s, sq_r.at[n], 2, i, f)
    for n, (i, f) in enumerate(tp_order[:-1]):
        tp_copy(sq_s, sq_r.at[n], 2, i, f).wait_recv()
        squares = squares + sq_r[n][0:1, :]
    inv_col = to_col(lax.rsqrt(squares * (1.0 / width) + norm_eps))
    for q in range(ns):
        inv_s[q] = jnp.broadcast_to(to_row(inv_col, inv_s.shape[2], q * rows), inv_s.shape[1:])
    inv_copies = {}
    for offset in far_first:
        inv_copies[offset] = ep_start(
            inv_s.at[offset // nch], inv_r.at[offset], 2, offset, offset
        )
    inv_r[0] = inv_s[0]
    normed = (gained * inv_col).astype(BF16)

    def first_step(product, s_ref, r_ref, o_ref, kind, h):
        s_ref[...] = product(pl.multiple_of((1 - me_c) * h, 128)).astype(BF16)
        tp_start(s_ref, r_ref, kind, 0, 1)
        o_ref[...] = product(pl.multiple_of(me_c * h, 128))

    def second_step(s_ref, r_ref, o_ref, ys_ref, yr_ref, kind):
        tp_copy(s_ref, r_ref, kind, 0, 1).wait_recv()
        total = o_ref[...] + r_ref[...].astype(F32)
        o_ref[...] = total
        ys_ref[...] = total.astype(BF16)
        for i in range(1, ny):
            tp_start(ys_ref, yr_ref.at[i], kind + 1, i, 0)

    def third_step(o_ref, ys_ref, yr_ref, in_ref, kind, h, scale):
        total = o_ref[...]
        for i in range(1, ny):
            tp_copy(ys_ref, yr_ref.at[i], kind + 1, i, 0).wait_recv()
            total = total + yr_ref[i].astype(F32)
        if scale is not None:
            total = total * scale
        in_ref[me_c] = (silu(total[:, 0:h]) * total[:, h : 2 * h]).astype(BF16)
        tp_start(in_ref.at[me_c], in_ref.at[me_c], kind + 2, 0, 1)

    def fourth_step(in_ref, kind):
        sib = 1 - me_c
        tp_copy(in_ref.at[sib], in_ref.at[sib], kind + 2, 0, 1).wait_recv()

    ready(i_sg)
    ready(i_su)

    def shared_half(at):
        gate = dot(normed, sg[:, pl.ds(at, hfs)])
        return jnp.concatenate([gate, dot(normed, su[:, pl.ds(at, hfs)])], 1)

    first_step(shared_half, hs, hr, ho, 4, hfs)

    def routed_first(p):
        chosen = dot(pick[p], xr[p].reshape(lanes, cols))
        parts = [chosen[a:b].astype(BF16) for a, b in bands(local, per)]

        def routed_half(at):
            return join_bands(
                [
                    jnp.concatenate(
                        [
                            dot(parts[e], eg[e, :, pl.ds(at, hf)]),
                            dot(parts[e], eu[e, :, pl.ds(at, hf)]),
                        ],
                        1,
                    )
                    for e in range(local)
                ],
                per,
            )

        first_step(routed_half, es.at[p], er.at[p], eo.at[p], 7 + 3 * p, hf)

    def routed_third(p):
        for offset in range(p, ep, nch):
            if offset:
                inv_copies[offset].wait_recv()
        inv = inv_r[p][0:1, 0:lanes]
        for q in range(1, ns):
            inv = inv + inv_r[q * nch + p][0:1, 0:lanes]
        scale = jnp.sum(pick[p].astype(F32) * inv, -1, keepdims=True)
        third_step(eo.at[p], ys.at[p], yr.at[p], inner.at[p], 7 + 3 * p, hf, scale)

    back_copies = {}

    def routed_back(p):
        fourth_step(inner.at[p], 7 + 3 * p)
        low, high = inner[p, 0].astype(F32), inner[p, 1].astype(F32)
        answer = join_bands(
            [
                dot(low[a:b].astype(BF16), ed[e, 0:hf, :])
                + dot(high[a:b].astype(BF16), ed[e, hf:ff, :])
                for e, (a, b) in enumerate(bands(local, per))
            ],
            per,
        ).astype(BF16)
        returned = dot(give_hi[p], answer) + dot(give_lo[p], answer)
        bs[p] = returned.astype(BF16).reshape(ns, rows, cols)
        for offset in [o for o in far_first if o % nch == p]:
            back_copies[offset] = ep_start(
                bs.at[p, offset // nch], br.at[offset], 3, offset, ep - offset
            )

    ready(i_eg)
    ready(i_eu)
    for p in range(nch):
        for offset in range(p, ep, nch):
            if offset:
                x_copies[offset].wait_recv()
        routed_first(p)
        if p == 0:
            second_step(hs, hr, ho, hys, hyr, 4)
        else:
            third_step(ho, hys, hyr, hinner, 4, hfs, None)
        second_step(es.at[p], er.at[p], eo.at[p], ys.at[p], yr.at[p], 7 + 3 * p)
    if nch == 1:
        third_step(ho, hys, hyr, hinner, 4, hfs, None)
    ready(i_sd)
    ready(i_ed)
    for p in range(nch):
        routed_third(p)
        if p == nch - 1:
            fourth_step(hinner, 4)
            mixture = dot(hinner[0], sd[0:hfs, :]) + dot(hinner[1], sd[hfs:fs, :])
        routed_back(p)
    last = res_scale * normed.astype(F32) + mixture + bs[0, 0].astype(F32)
    for offset in [o for o in far_first[::-1] if o % nch == 0] + [o for o in far_first if o % nch]:
        back_copies[offset].wait_recv()
        last = last + br[offset].astype(F32)

    mean = jnp.mean(last, -1, keepdims=True)
    center = last - mean
    moment = jnp.sum(center * center, -1, keepdims=True)
    spread_r = ln_s.shape[1]
    mean_row = to_row(mean, spread_r, 0)
    moment_row = to_row(moment, spread_r, 0)
    ln_s[...] = jnp.where(iota((8, spread_r), 0) == 0, mean_row, moment_row)
    for n, (i, f) in enumerate(tp_order[:-1]):
        tp_start(ln_s, ln_r.at[n], 3, i, f)
    means = [mean_row]
    for n, (i, f) in enumerate(tp_order[:-1]):
        tp_copy(ln_s, ln_r.at[n], 3, i, f).wait_recv()
        tile = ln_r[n]
        means.append(tile[0:1, :])
        moment_row = moment_row + tile[1:2, :]
    total = sum(means) * (1.0 / tp)
    for m in means:
        moment_row = moment_row + cols * (m - total) * (m - total)
    scale = lax.rsqrt(moment_row * (1.0 / width) + norm_eps)
    out[...] = ((last - to_col(total)) * to_col(scale) * g2_v[...]).astype(BF16)
    for copy in sent:
        copy.wait_send()


def per_device(
    tokens,
    state,
    w_query,
    w_key,
    w_value,
    w_outgate,
    decay_down,
    decay_up,
    decay_bias,
    head_gain,
    w_output,
    norm1_gain,
    route_ids,
    route_weight,
    exp_gate,
    exp_up,
    exp_down,
    sh_gate,
    sh_up,
    sh_down,
    norm2_gain,
):
    rows, width = tokens.shape
    heads, kdim, vdim = state.shape[1:]
    tp, ep = lax.axis_size("tp"), lax.axis_size("ep")
    cols = width // tp
    top = route_ids.shape[1]
    local = exp_gate.shape[0]
    cap = max(2, rows * top // (local * ep) + 1)
    ff, fs = exp_gate.shape[2], sh_gate.shape[1]
    nch = 2 if ep % 2 == 0 else 1
    ns, ny = ep // nch, tp // 2
    slots = local * ns * cap
    lanes, lanes_pad = ns * rows, pad_to(ns * rows, 128)
    rows_pad = pad_to(rows, 128)
    r16 = pad_to(3 * local, 16)
    chunks = 4
    dims = (rows, heads, kdim, vdim, width, cols, tp, ep, local, cap, top, ff, fs, chunks, nch, r16)
    n_loads = 10 + 1 + chunks + 4 + tp + 6
    vm = pltpu.VMEM
    smalls = (
        tokens,
        decay_down.T,
        decay_up,
        decay_bias[None, :],
        head_gain[None, :],
        norm1_gain[None, :],
        route_ids.T,
        route_weight.T,
        norm2_gain[None, :],
    )
    return pl.pallas_call(
        functools.partial(kernel, dims),
        out_shape=pltpu.VMEM((rows, cols), BF16),
        in_specs=[pl.BlockSpec(memory_space=pl.ANY)] * 21,
        out_specs=pl.BlockSpec(memory_space=pltpu.VMEM),
        scratch_shapes=[vm(a.shape, a.dtype) for a in smalls]
        + [
            vm(state.shape, F32),
            vm(w_query.shape, BF16),
            vm(w_key.shape, BF16),
            vm(w_value.shape, BF16),
            vm(w_outgate.shape, BF16),
            vm((tp, w_output.shape[0], cols), BF16),
            vm(exp_gate.shape, BF16),
            vm(exp_up.shape, BF16),
            vm(exp_down.shape, BF16),
            vm(sh_gate.shape, BF16),
            vm(sh_up.shape, BF16),
            vm(sh_down.shape, BF16),
            vm((rows, heads * kdim), F32),
            vm((rows, pad_to(heads, 8), vdim), F32),
            vm((rows, heads * vdim), BF16),
            vm((ep, r16, rows), F32),
            vm((ep, r16, lanes_pad), BF16),
            vm((ep, r16, lanes_pad), BF16),
            vm((nch, slots, lanes), BF16),
            vm((nch, lanes, slots), BF16),
            vm((nch, lanes, slots), BF16),
            vm((tp, rows, cols), BF16),
            vm((tp, rows, cols), BF16),
            vm((8, rows_pad), F32),
            vm((tp, 8, rows_pad), F32),
            vm((8, rows_pad), F32),
            vm((tp, 8, rows_pad), F32),
            vm((8, rows_pad), F32),
            vm((tp, 8, rows_pad), F32),
            vm((ns, 8, lanes_pad), F32),
            vm((ep, 8, lanes_pad), F32),
            vm((rows, cols), BF16),
            vm((nch, ns, rows, cols), BF16),
            vm((nch, slots, ff), BF16),
            vm((nch, slots, ff), BF16),
            vm((nch, slots, ff), F32),
            vm((nch, slots, ff), BF16),
            vm((nch, ny, slots, ff), BF16),
            vm((nch, 2, slots, ff // 2), BF16),
            vm((rows, fs), BF16),
            vm((rows, fs), BF16),
            vm((rows, fs), F32),
            vm((rows, fs), BF16),
            vm((ny, rows, fs), BF16),
            vm((2, rows, fs // 2), BF16),
            vm((nch, ns, rows, cols), BF16),
            vm((ep, rows, cols), BF16),
            pltpu.SemaphoreType.DMA((n_loads,)),
            pltpu.SemaphoreType.DMA((13, tp)),
            pltpu.SemaphoreType.DMA((13, tp)),
            pltpu.SemaphoreType.DMA((4, ep)),
            pltpu.SemaphoreType.DMA((4, ep)),
        ],
        compiler_params=pltpu.CompilerParams(
            collective_id=0, has_side_effects=True, vmem_limit_bytes=60 * 1024 * 1024
        ),
        name="layer",
    )(
        *smalls,
        state,
        w_query,
        w_key,
        w_value,
        w_outgate,
        w_output,
        exp_gate,
        exp_up,
        exp_down,
        sh_gate,
        sh_up,
        sh_down,
    )


def solution(mesh):
    in_specs = (
        P("ep", None),
        P("ep", "tp", None, None),
        P(None, "tp"),
        P(None, "tp"),
        P(None, "tp"),
        P(None, "tp"),
        P(),
        P(None, "tp"),
        P("tp"),
        P(),
        P("tp", None),
        P("tp"),
        P("ep", None),
        P("ep", None),
        P("ep", "tp", None),
        P("ep", "tp", None),
        P("ep", None, "tp"),
        P("tp", None),
        P("tp", None),
        P(None, "tp"),
        P("tp"),
    )
    out_specs = P("ep", "tp")
    return jax.shard_map(
        per_device, mesh=mesh, in_specs=in_specs, out_specs=out_specs, check_vma=False
    )
```

time: 48.2 us -> 41.5 us (0.86)
  Pallas kernels: 46.6 us -> 40.8 us
  local copies, waits for them, and re-layouts: 1.35 us -> 0.61 us
    pallas_call x1, Pallas kernels: 46.6 us -> 40.8 us  [per_device(): pl.pallas_call(functools.partial(kernel, dims), out_shape=pltpu.VMEM((row...]
    unnamed x1, local copies, waits for them, and re-layouts: 1.35 us -> 0.61 us
where the time goes in v1:
time: 41.5 us; the launch traced here: 41.4 us
  Pallas kernels  40.8 us (98%)
  local copies, waits for them, and re-layouts  0.61 us (1%)
    pallas_call x1, Pallas kernels, per_device(): pl.pallas_call(functools.partial(kernel, dims), out_shape=pltpu.VMEM((row...  40.8 us

profile of v1, /device:TPU:0, one launch (start us, length us, event | category | flops | bytes accessed | tf_op | source)
XLA Modules:
  0.0 41.4 jit_solution(7707982003901916667)
XLA Ops:
  0.0 40.8 %layer.1 = bf16[24,512]{1,0:T(8,128)(2,1)S(1)} custom-call(bf16[24,2048]{1,0:T(8,128)(2,1)} %refs_0_.1, bf16[16,2048]{1,0:T(8,128)(2,1)} %bitcast.7, bf16[16,512]{1,0:T(8,128)(2,1)} %refs_2_.1, f32[1,512]{1,0:T(1,128)} %bitcast.10, f32[1,256]{1,0:T(1,128)} %bitcast.13, f32[1,512]{1,0:T(1,128)} %bitcast.11, s32[6,24]{1,0:T(8,128)} %bitcast.8, ...), custom_call_target="tpu_custom_call" | custom-call | tf_op jit(solution)/shard_map/layer/pallas_call | solution.py:541
  40.8 0.6 %copy.23 = bf16[24,512]{1,0:T(8,128)(2,1)} copy(bf16[24,512]{1,0:T(8,128)(2,1)S(1)} %layer.1) | data formatting | bytes 49152
